TPU v7x, 32 devices: a whole 2x2x4 slice. The times are simulated.
32 devices in a mesh: sp: 4 (over z), fs: 4 (over y, x), tp: 2 (over core).
Axes of the slice: x: 2, y: 2, z: 4, core: 2. Of those that a mesh axis runs over, the one named last changes fastest.
Arguments:
- layer_entering_vectors: bfloat16 [4, 1024, 2048], P('fs', ('sp', 'tp')), may hold values from -6 to 6
- entering_rms_coefficients: float32 [2048], replicated, may hold values from 0.1 to 1.9
- question_projection: bfloat16 [2048, 1536], P('fs', 'tp'), may hold values from -0.125 to 0.125
- compressing_projection: bfloat16 [2048, 256], P('fs'), may hold values from -0.125 to 0.125
- spinning_address_projection: bfloat16 [2048, 32], P('fs'), may hold values from -0.125 to 0.125
- compact_rms_coefficients: float32 [256], replicated, may hold values from 0.1 to 1.9
- compact_to_plain_address: bfloat16 [256, 1024], P(None, 'tp'), may hold values from -0.375 to 0.375
- compact_to_content: bfloat16 [256, 1024], P(None, 'tp'), may hold values from -0.375 to 0.375
- question_rms_coefficients: float32 [96], replicated, may hold values from 0.7 to 6
- address_rms_coefficients: float32 [96], replicated, may hold values from 0.7 to 6
- acceptance_projection: bfloat16 [2048, 1024], P('fs', 'tp'), may hold values from -0.125 to 0.125
- state_address_projection: bfloat16 [2048, 1024], P('fs', 'tp'), may hold values from -0.125 to 0.125
- state_content_projection: bfloat16 [2048, 1024], P('fs', 'tp'), may hold values from -0.125 to 0.125
- fading_first_lowrank: bfloat16 [2048, 128], replicated, may hold values from -0.125 to 0.125
- fading_second_lowrank: bfloat16 [128, 1024], P(None, 'tp'), may hold values from -0.375 to 0.375
- fading_channel_bias: float32 [1024], P('tp'), may hold values from -20 to -2
- fading_speed_multiplier: float32 [4, 16, 1024], P('fs', 'tp', 'sp'), may hold values from 0.5 to 2, as said below
- fading_extra_exponent: float32 [4, 16, 1024], P('fs', 'tp', 'sp'), may hold values from -0.7 to 0
- adaptation_first_lowrank: bfloat16 [2048, 128], replicated, may hold values from -0.125 to 0.125
- adaptation_second_lowrank: bfloat16 [128, 1024], P(None, 'tp'), may hold values from -0.5 to 0.5
- adaptation_channel_bias: float32 [1024], P('tp'), may hold values from -12 to -1
- present_token_coefficients: float32 [16, 64], P('tp'), may hold values from -1.5 to 1.5
- branch_rms_coefficients: float32 [1024], P('tp'), may hold values from 0.1 to 1.9
- softmax_merge_projection: bfloat16 [1024, 2048], P('tp', 'fs'), may hold values from -0.1875 to 0.1875
- state_merge_projection: bfloat16 [1024, 2048], P('tp', 'fs'), may hold values from -0.1875 to 0.1875
Outputs:
- mixed: bfloat16 [4, 1024, 2048], P('fs', ('sp', 'tp'))
- log_total: float32 [4, 16, 1024], P('fs', 'tp', 'sp')
Inputs may be any that keep to these rules, and one draw needn't show every extreme that they name: `fading_speed_multiplier`: constant over aligned blocks of 256 positions.
All inputs are finite; a program needn't handle non-finite values.
Results may differ from a plain program's by a relative error of at most 0.015.
Values may be sent and summed in bfloat16 or wider, within the bound.
A program may use at most 128 MiB of HBM per device.

v0:
```python
import jax
import jax.numpy as jnp
from jax import lax
from jax.sharding import PartitionSpec as P

NOPE = 64
ROPE = 32
VHEAD = 64
BRANCH_CHANNELS = 64
TOK_DEV = 256


norm_epsilon = 1e-06
group_epsilon = 0.00064
highest = lax.Precision.HIGHEST


def passed_along(block, axis, distance):
    devices = range(lax.axis_size(axis))
    route = [(i - distance, i) for i in devices if i - distance in devices]
    return lax.ppermute(block, axis, route)


def rms_rows(values, gain):
    floats = values.astype(jnp.float32)
    return (
        floats * lax.rsqrt(jnp.mean(floats * floats, axis=-1, keepdims=True) + norm_epsilon) * gain
    )


def rotate(values, positions):
    half = values.shape[-1] // 2
    inverse = 10000.0 ** (-jnp.arange(half, dtype=jnp.float32) / half)
    angle = positions.astype(jnp.float32)[:, None] * inverse[None, :]
    cosine = jnp.cos(angle)[:, None, :]
    sine = jnp.sin(angle)[:, None, :]
    first = values[..., :half]
    second = values[..., half:]
    return jnp.concatenate(
        [first * cosine - second * sine, second * cosine + first * sine], axis=-1
    )


def finish(stacked, gain, positions):
    normed = rms_rows(stacked, gain)
    return jnp.concatenate(
        [normed[..., :NOPE], rotate(normed[..., NOPE:], positions)], axis=-1
    ).astype(jnp.bfloat16)


def matmul(left, right):
    return jnp.dot(left, right, preferred_element_type=jnp.float32)


def pair_decay(later, earlier, mask):
    differ = later[:, :, :, None, :] - earlier[:, :, None, :, :]
    return jnp.exp(jnp.where(mask[None, None, :, :, None], differ, -jnp.inf))


def shards(
    layer_entering_vectors,
    entering_rms_coefficients,
    question_projection,
    compressing_projection,
    spinning_address_projection,
    compact_rms_coefficients,
    compact_to_plain_address,
    compact_to_content,
    question_rms_coefficients,
    address_rms_coefficients,
    acceptance_projection,
    state_address_projection,
    state_content_projection,
    fading_first_lowrank,
    fading_second_lowrank,
    fading_channel_bias,
    fading_speed_multiplier,
    fading_extra_exponent,
    adaptation_first_lowrank,
    adaptation_second_lowrank,
    adaptation_channel_bias,
    present_token_coefficients,
    branch_rms_coefficients,
    softmax_merge_projection,
    state_merge_projection,
):
    gathered = (
        lax.all_gather(question_projection, "fs", axis=0, tiled=True),
        lax.all_gather(compressing_projection, "fs", axis=0, tiled=True),
        lax.all_gather(spinning_address_projection, "fs", axis=0, tiled=True),
        lax.all_gather(acceptance_projection, "fs", axis=0, tiled=True),
        lax.all_gather(state_address_projection, "fs", axis=0, tiled=True),
        lax.all_gather(state_content_projection, "fs", axis=0, tiled=True),
    )
    widths = [stream_position_entry.shape[1] for stream_position_entry in gathered] + [
        fading_first_lowrank.shape[1],
        adaptation_first_lowrank.shape[1],
    ]
    joined = jnp.concatenate(
        list(gathered) + [fading_first_lowrank, adaptation_first_lowrank], axis=1
    )
    bounds = [0]
    for width in widths:
        bounds.append(bounds[-1] + width)
    normed = rms_rows(
        lax.all_gather(layer_entering_vectors, "tp", axis=1, tiled=True)[0],
        entering_rms_coefficients,
    ).astype(jnp.bfloat16)
    projected = matmul(normed, joined).astype(jnp.bfloat16)[None][0]
    columns = [projected[:, bounds[index] : bounds[index + 1]] for index in range(len(widths))]
    query, latent, rope_key, recept_in, rkey_in, rvalue_in, decay_in, rate_low = columns
    row_count = projected.shape[0]
    attn_heads = compact_to_plain_address.shape[1] // NOPE
    qk_size = NOPE + ROPE
    own_positions = lax.axis_index("sp") * row_count + jnp.arange(row_count, dtype=jnp.int32)
    last_position = lax.axis_index("sp") * row_count + row_count - 1
    latent_normed = rms_rows(latent, compact_rms_coefficients).astype(jnp.bfloat16)
    query_ready = finish(
        query.reshape(row_count, attn_heads, qk_size), question_rms_coefficients, own_positions
    )
    scale = qk_size ** (-0.5)
    start_carry = (
        jnp.full((attn_heads, row_count), -jnp.inf, jnp.float32),
        jnp.zeros((attn_heads, row_count), jnp.float32),
        jnp.zeros((attn_heads, row_count, VHEAD), jnp.float32),
    )
    length_here = latent_normed.shape[0]
    key_nope = (
        matmul(latent_normed, compact_to_plain_address)
        .astype(jnp.bfloat16)
        .reshape(length_here, attn_heads, NOPE)
    )
    values_here = (
        matmul(latent_normed, compact_to_content)
        .astype(jnp.bfloat16)
        .reshape(length_here, attn_heads, VHEAD)
    )
    key_stack = jnp.concatenate(
        [key_nope, jnp.broadcast_to(rope_key[:, None, :], (length_here, attn_heads, ROPE))], axis=-1
    )
    key_ready = finish(key_stack, address_rms_coefficients, own_positions)
    carry = start_carry
    key_rows = lax.all_gather(key_ready, "sp", axis=0, tiled=True)
    length_here = key_rows.shape[0]
    block = TOK_DEV
    blocks = length_here // block
    keys_blocked = key_rows.reshape(blocks, block, attn_heads, qk_size)
    values_blocked = lax.all_gather(values_here, "sp", axis=0, tiled=True).reshape(
        blocks, block, attn_heads, VHEAD
    )

    def visit(state, inputs):
        key_block, value_block, index = inputs
        block_start = index * block

        def compute(running):
            running_max, running_total, running_sum = running
            scores = (
                jnp.einsum(
                    "qhd,khd->hqk", query_ready, key_block, preferred_element_type=jnp.float32
                )
                * scale
            )
            key_positions = block_start + jnp.arange(block, dtype=jnp.int32)
            allowed = key_positions[None, :] <= own_positions[:, None]
            scores = jnp.where(allowed[None], scores, -jnp.inf)
            new_max = jnp.maximum(running_max, jnp.max(scores, axis=-1))
            safe_max = jnp.where(jnp.isfinite(new_max), new_max, 0.0)
            weights = jnp.exp(scores - safe_max[..., None])
            factor = jnp.exp(running_max - safe_max)
            new_total = running_total * factor + jnp.sum(weights, axis=-1)
            new_sum = running_sum * factor[..., None] + jnp.einsum(
                "hqk,khd->hqd",
                weights.astype(jnp.bfloat16),
                value_block,
                preferred_element_type=jnp.float32,
            )
            return (new_max, new_total, new_sum)

        def keep(running):
            return running

        return (lax.cond(block_start > last_position, keep, compute, state), None)

    carry, _ = lax.scan(
        visit, carry, (keys_blocked, values_blocked, jnp.arange(blocks, dtype=jnp.int32))
    )
    final_max, final_total, final_sum = carry
    attended = (final_sum / final_total[..., None]).astype(jnp.bfloat16)
    attended = jnp.transpose(attended, (1, 0, 2)).reshape(row_count, attn_heads * VHEAD)
    log_total = final_max + jnp.log(final_total)
    recurrent_heads = fading_second_lowrank.shape[1] // BRANCH_CHANNELS

    def heads(values):
        return values.astype(jnp.float32).reshape(row_count, recurrent_heads, BRANCH_CHANNELS)

    acceptance_tokens_flat = heads(recept_in)
    state_address = heads(rkey_in)
    state_content = heads(rvalue_in)
    decay_low = jnp.tanh(decay_in.astype(jnp.float32)).astype(jnp.bfloat16)
    rate_logarithm = (
        -jax.nn.softplus(-(fading_channel_bias + matmul(decay_low, fading_second_lowrank))) - 0.5
    )
    log_decay = (
        -jnp.exp(rate_logarithm).reshape(row_count, recurrent_heads, BRANCH_CHANNELS)
        * jnp.transpose(fading_speed_multiplier[0])[:, :, None]
        + jnp.transpose(fading_extra_exponent[0])[:, :, None]
    )
    learn = jax.nn.sigmoid(
        adaptation_channel_bias + matmul(rate_low, adaptation_second_lowrank)
    ).reshape(row_count, recurrent_heads, BRANCH_CHANNELS)
    unit = state_address * lax.rsqrt(
        jnp.sum(state_address * state_address, axis=-1, keepdims=True) + 1e-06
    )
    span = 16
    spans = row_count // span

    def by_span(values):
        return jnp.transpose(
            values.reshape(spans, span, recurrent_heads, BRANCH_CHANNELS), (0, 2, 1, 3)
        )

    cum_log = jnp.cumsum(by_span(log_decay), axis=2)
    prev_log = cum_log - by_span(log_decay)
    toward = -by_span(unit)
    remove = by_span(unit * learn)
    span_key = by_span(state_address)
    span_value = by_span(state_content)
    span_recept = by_span(acceptance_tokens_flat)
    rows_index = jnp.arange(span, dtype=jnp.int32)
    strict = rows_index[:, None] > rows_index[None, :]
    inclusive = rows_index[:, None] >= rows_index[None, :]
    before = pair_decay(prev_log, cum_log, strict)
    upto = pair_decay(cum_log, cum_log, inclusive)
    remove_before = jnp.einsum("nhtsk,nhsk,nhtk->nhts", before, remove, toward, precision=highest)
    key_before = jnp.einsum("nhtsk,nhsk,nhtk->nhts", before, span_key, toward, precision=highest)
    remove_upto = jnp.einsum("nhtsk,nhsk,nhtk->nhts", upto, remove, span_recept, precision=highest)
    key_upto = jnp.einsum("nhtsk,nhsk,nhtk->nhts", upto, span_key, span_recept, precision=highest)
    system = jnp.eye(span, dtype=jnp.float32) - remove_before
    start_coef = jnp.exp(prev_log) * toward
    lead_coef = lax.linalg.triangular_solve(
        system, start_coef, left_side=True, lower=True, unit_diagonal=True
    )
    lead_free = lax.linalg.triangular_solve(
        system,
        jnp.einsum("nhts,nhsv->nhtv", key_before, span_value, precision=highest),
        left_side=True,
        lower=True,
        unit_diagonal=True,
    )
    read_coef_span = jnp.exp(cum_log) * span_recept + jnp.einsum(
        "nhts,nhsk->nhtk", remove_upto, lead_coef, precision=highest
    )
    read_free_span = jnp.einsum(
        "nhts,nhsv->nhtv", remove_upto, lead_free, precision=highest
    ) + jnp.einsum("nhts,nhsv->nhtv", key_upto, span_value, precision=highest)
    tail = jnp.exp(cum_log[:, :, -1:, :] - cum_log)
    remove_tail = remove * tail
    key_tail = span_key * tail
    identity = jnp.broadcast_to(
        jnp.eye(BRANCH_CHANNELS, dtype=jnp.float32),
        (recurrent_heads, BRANCH_CHANNELS, BRANCH_CHANNELS),
    )
    span_map = jnp.exp(cum_log[:, :, -1, :])[:, :, None, :] * identity[None] + jnp.einsum(
        "nhsk,nhsj->nhkj", lead_coef, remove_tail, precision=highest
    )
    span_add = jnp.einsum(
        "nhsv,nhsj->nhvj", lead_free, remove_tail, precision=highest
    ) + jnp.einsum("nhsv,nhsj->nhvj", span_value, key_tail, precision=highest)

    def advance(carry, inputs):
        local_now, transfer_now = carry
        map_here, add_here, coef_here, free_here = inputs
        read_local = free_here + jnp.einsum("hvk,htk->htv", local_now, coef_here, precision=highest)
        read_along = jnp.einsum("hjk,htk->htj", transfer_now, coef_here, precision=highest)
        local_next = jnp.einsum("hvk,hkj->hvj", local_now, map_here, precision=highest) + add_here
        transfer_next = jnp.einsum("hik,hkj->hij", transfer_now, map_here, precision=highest)
        return ((local_next, transfer_next), (read_local, read_along))

    (local_state, transfer), (read_free, read_along) = lax.scan(
        advance,
        (jnp.zeros_like(identity), identity),
        (span_map, span_add, read_coef_span, read_free_span),
    )
    read_free = jnp.transpose(read_free, (0, 2, 1, 3)).reshape(
        row_count, recurrent_heads, BRANCH_CHANNELS
    )
    read_along = jnp.transpose(read_along, (0, 2, 1, 3)).reshape(
        row_count, recurrent_heads, BRANCH_CHANNELS
    )

    def turn(index, incoming):
        outgoing = jnp.einsum("hij,hjk->hik", incoming, transfer, precision=highest) + local_state
        return passed_along(outgoing.astype(jnp.bfloat16), "sp", 1).astype(outgoing.dtype)

    entering = lax.fori_loop(0, lax.axis_size("sp") - 1, turn, jnp.zeros_like(local_state))
    read = read_free + jnp.einsum("hvk,thk->thv", entering, read_along, precision=highest)
    center = jnp.mean(read, axis=-1, keepdims=True)
    spread = jnp.mean(jnp.square(read - center), axis=-1, keepdims=True)
    retrieved_rescaled = (
        (read - center)
        * lax.rsqrt(spread + group_epsilon)
        * branch_rms_coefficients.reshape(recurrent_heads, BRANCH_CHANNELS)
    )
    present_token_term = (
        jnp.sum(
            acceptance_tokens_flat * state_address * present_token_coefficients,
            axis=-1,
            keepdims=True,
        )
        * state_content
    )
    state_branch_result = (
        (retrieved_rescaled + present_token_term)
        .reshape(row_count, recurrent_heads * BRANCH_CHANNELS)
        .astype(jnp.bfloat16)
    )
    out_attn_full, out_rec_full = (
        lax.all_gather(softmax_merge_projection, "fs", axis=1, tiled=True),
        lax.all_gather(state_merge_projection, "fs", axis=1, tiled=True),
    )
    mixed = lax.psum_scatter(
        (matmul(attended, out_attn_full) + matmul(state_branch_result, out_rec_full)).astype(
            jnp.bfloat16
        ),
        "tp",
        scatter_dimension=0,
        tiled=True,
    )
    return (mixed[None], log_total[None])


def solution(mesh):
    placed = (
        P("fs", ("sp", "tp"), None),
        P(),
        P("fs", "tp"),
        P("fs", None),
        P("fs", None),
        P(),
        P(None, "tp"),
        P(None, "tp"),
        P(),
        P(),
        P("fs", "tp"),
        P("fs", "tp"),
        P("fs", "tp"),
        P(),
        P(None, "tp"),
        P("tp"),
        P("fs", "tp", "sp"),
        P("fs", "tp", "sp"),
        P(),
        P(None, "tp"),
        P("tp"),
        P("tp", None),
        P("tp"),
        P("tp", "fs"),
        P("tp", "fs"),
    )
    return jax.shard_map(
        shards,
        mesh=mesh,
        in_specs=placed,
        out_specs=(P("fs", ("sp", "tp"), None), P("fs", "tp", "sp")),
        check_vma=False,
    )
```

profile of v0, /device:TPU:0, one launch (start us, length us, event | category | flops | bytes accessed | tf_op | source)
XLA Modules:
  0.0 775.9 jit_solution(5312688305198085367)
XLA Ops:
  11.2 10.1 %all_gather.36 = bf16[2048,32]{0,1:T(8,128)(2,1)S(1)} all-gather(bf16[512,32]{0,1:T(8,128)(2,1)} %param.39), channel_id=1, replica_groups=mesh['sp'=4,'fs'=4,'tp'=2] {'fs'}, dimensions={0}, use_global_device_ids=true | all-gather | bytes 163840 | tf_op jit(solution)/shard_map/all_gather | solution.py:90
  23.2 27.6 %all-gather.15.cloned.1.call-done = bf16[2048,256]{1,0:T(8,128)(2,1)} async-done(((bf16[512,256]{1,0:T(8,128)(2,1)}), bf16[2048,256]{1,0:T(8,128)(2,1)}) %all-gather.15.cloned.1.call-update) | async-done | bytes 1048592 | tf_op jit(solution)/shard_map/all_gather | solution.py:89
  50.9 37.1 %all-gather.17.cloned.1.call-done = bf16[2048,512]{1,0:T(8,128)(2,1)} async-done(((bf16[512,512]{1,0:T(8,128)(2,1)}), bf16[2048,512]{1,0:T(8,128)(2,1)}) %all-gather.17.cloned.1.call-update) | async-done | bytes 2097168 | tf_op jit(solution)/shard_map/all_gather | solution.py:91
  87.9 36.9 %all-gather.19.cloned.1.call-done = bf16[2048,512]{1,0:T(8,128)(2,1)} async-done(((bf16[512,512]{1,0:T(8,128)(2,1)}), bf16[2048,512]{1,0:T(8,128)(2,1)}) %all-gather.19.cloned.1.call-update) | async-done | bytes 2097168 | tf_op jit(solution)/shard_map/all_gather | solution.py:92
  124.9 36.9 %all-gather.21.cloned.1.call-done = bf16[2048,512]{1,0:T(8,128)(2,1)} async-done(((bf16[512,512]{1,0:T(8,128)(2,1)}), bf16[2048,512]{1,0:T(8,128)(2,1)}) %all-gather.21.cloned.1.call-update) | async-done | bytes 2097168 | tf_op jit(solution)/shard_map/all_gather | solution.py:93
  161.8 45.6 %all-gather.13.cloned.1.call-done = bf16[2048,768]{1,0:T(8,128)(2,1)} async-done(((bf16[512,768]{1,0:T(8,128)(2,1)}), bf16[2048,768]{1,0:T(8,128)(2,1)}) %all-gather.13.cloned.1.call-update) | async-done | bytes 3145744 | tf_op jit(solution)/shard_map/all_gather | solution.py:88
  207.3 19.4 %concatenate.14 = bf16[2048,2848]{1,0:T(8,128)(2,1)} concatenate(bf16[2048,768]{1,0:T(8,128)(2,1)} %all-gather.13.cloned.1.call-done, bf16[2048,256]{1,0:T(8,128)(2,1)} %all-gather.15.cloned.1.call-done, bf16[2048,32]{1,0:T(8,128)(2,1)S(1)} %copy.65, bf16[2048,512]{1,0:T(8,128)(2,1)} %all-gather.17.cloned.1.call-done, bf16[2048,512]{1,0:T(8,128)(2,1)} %all-gather.19.cloned.1.call-done, ...), dimensions={1} | concatenate | bytes 23330816 | tf_op jit(solution)/shard_map/concatenate | solution.py:99
  226.7 9.4 %convolution_convert_fusion = bf16[256,2848]{0,1:T(8,128)(2,1)S(1)} fusion(bf16[2048,2848]{1,0:T(8,128)(2,1)} %concatenate.14, bf16[1,256,2048]{2,1,0:T(8,128)(2,1)S(1)} %copy-done.20, f32[2048]{0:T(1024)S(1)} %copy-done.46, f32[256]{0:T(256)S(1)} %add_rsqrt_fusion.5), kind=kOutput, calls=%fused_computation.90 | convolution fusion | flops 2989170688 | bytes 14181376 | tf_op jit(solution)/shard_map/dot_general | solution.py:52
  242.5 13.1 %reduce-scatter.2.cloned.1.call-start = ((), (), s32[]{:S(2)}) async-start(), calls=%async_computation.11 | async-start | bytes 1572864 | tf_op jit(solution)/shard_map/reduce_scatter | solution.py:322
  282.5 29.4 %fusion.48 = f32[16,8,16,1,16]{4,3,2,1,0:T(1,128)} fusion(f32[16,8,16,64]{3,2,1,0:T(8,128)S(1)} %copy.77, f32[16,8,16,64]{3,2,1,0:T(8,128)S(1)} %copy-done.21, f32[16,8,16,64]{3,2,1,0:T(8,128)S(1)} %copy.75, pred[16,16]{1,0:T(8,128)(4,1)S(1)} %copy-done.41, f32[16,8,16,64,1]{3,1,2,0,4:T(8,128)S(1)} %negate_bitcast_fusion), kind=kOutput, calls=%fused_computation.61 | convolution fusion | flops 31457280 | bytes 2228480 | tf_op jit(solution)/shard_map/nhtsk,nhsk,nhtk->nhts/dot_general | solution.py:235
  311.9 30.0 %fusion.46 = f32[16,8,16,1,16]{4,3,2,1,0:T(1,128)} fusion(f32[16,8,16,64]{3,2,1,0:T(8,128)S(1)} %copy.82, f32[16,8,16,64]{3,2,1,0:T(8,128)S(1)} %copy-done.21, f32[16,8,16,64]{3,2,1,0:T(8,128)S(1)} %copy.75, pred[16,16]{1,0:T(8,128)(4,1)S(1)} %copy-done.41, f32[16,8,16,64,1]{3,1,2,0,4:T(8,128)S(1)} %negate_bitcast_fusion), kind=kOutput, calls=%fused_computation.59 | convolution fusion | flops 31457280 | bytes 2228480 | tf_op jit(solution)/shard_map/nhtsk,nhsk,nhtk->nhts/dot_general | solution.py:236
  342.3 18.6 %fusion.44 = f32[16,8,16,1,16]{4,3,2,1,0:T(1,128)} fusion(f32[16,8,16,64]{3,2,1,0:T(8,128)} %copy.76, f32[16,8,16,64]{3,2,1,0:T(8,128)} %copy-done.23, pred[16,16]{1,0:T(8,128)(4,1)S(1)} %copy-done.40, bf16[16,8,16,64,1]{3,1,2,0,4:T(8,128)(2,1)S(1)} %bitcast.234), kind=kOutput, calls=%fused_computation.57 | convolution fusion | flops 31457280 | bytes 1442048 | tf_op jit(solution)/shard_map/nhtsk,nhsk,nhtk->nhts/dot_general | solution.py:237
  361.0 17.4 %fusion.42 = f32[16,8,16,1,16]{4,3,2,1,0:T(1,128)} fusion(f32[16,8,16,64]{3,2,1,0:T(8,128)S(1)} %copy-done.22, f32[16,8,16,64]{3,2,1,0:T(8,128)S(1)} %copy-done.25, pred[16,16]{1,0:T(8,128)(4,1)S(1)} %copy-done.40, bf16[16,8,16,64,1]{3,1,2,0,4:T(8,128)(2,1)S(1)} %bitcast.235), kind=kOutput, calls=%fused_computation.55 | convolution fusion | flops 31457280 | bytes 1442048 | tf_op jit(solution)/shard_map/nhtsk,nhsk,nhtk->nhts/dot_general | solution.py:238
  379.5 160.7 %custom-call.6 = f32[16,8,1,16,16]{3,4,2,1,0:T(8,128)} custom-call(f32[16,8,1,16,16]{4,3,2,1,0:T(8,128)} %add_bitcast_fusion), custom_call_target="InvertDiagBlocksLowerTriangular" | custom-call | tf_op jit(solution)/shard_map/triangular_solve/custom-call.1 | solution.py:241
  541.4 3.5 fusion.90
  548.8 8.3 %fusion.100 = f32[16,8,64,64]{3,2,1,0:T(8,128)} fusion(f32[16,8,16,64]{3,2,1,0:T(8,128)S(1)} %fusion.88, f32[16,8,16,64]{3,1,2,0:T(8,128)S(1)} %get-tuple-element.388), kind=kOutput, calls=%fused_computation.137 | convolution fusion | flops 100663296 | bytes 3145728 | tf_op jit(solution)/shard_map/nhsv,nhsj->nhvj/dot_general | solution.py:267
  563.6 8.5 %multiply_add_fusion.1 = f32[16,8,64,64]{3,2,1,0:T(8,128)} fusion(f32[16,8,16,64]{3,2,1,0:T(8,128)S(1)} %fusion.90, f32[64,64]{1,0:T(8,128)S(1)} %copy-done.29, f32[16,8,64]{2,1,0:T(8,128)S(1)} %copy-done.30, f32[16,8,16,64]{3,1,2,0:T(8,128)S(1)} %get-tuple-element.388), kind=kOutput, calls=%fused_computation.89 | convolution fusion | flops 101711872 | bytes 3194880 | tf_op jit(solution)/shard_map/nhsk,nhsj->nhkj/dot_general | solution.py:264
  574.5 3.7 convolution_add_fusion.4
  579.0 126.5 %while.44 = (s32[]{:T(128)}, f32[8,64,64]{1,2,0:T(8,128)S(1)}, f32[8,64,64]{1,2,0:T(8,128)S(1)}, f32[16,8,16,64]{3,2,1,0:T(8,128)}, f32[16,8,16,64]{3,2,1,0:T(8,...) while((s32[]{:T(128)}, f32[8,64,64]{1,2,0:T(8,128)S(1)}, ...), condition=%wide.region_13.15_spmd.clone, body=%wide.region_12.14_spmd.clone.sunk | while | flops 63021056 | bytes 2787979 | solution.py:280
  710.5 21.0 %while.45 = (s32[]{:T(128)}, f32[8,64,64]{2,1,0:T(8,128)S(1)}, f32[8,64,64]{2,1,0:T(8,128)S(1)}, f32[8,64,64]{2,1,0:T(8,128)S(1)}, s32[]{:T(128)}, /*index=5*/s32[]{:T(128)}) while((s32[]{:T(128)}, f32[8,64,64]{2,1,0:T(8,128)S(1)}, f32[8,64,64]{2,1,0:T(8,128)S(1)}, f32[8,64,64]{2,1,0:T(8,128)S(1)}, s32[]{:T(128)}, ...), condition=%wide.region_15.17_spmd.clone, body=%wide.region_14.16_spmd.clone.sunk | while | flops 25296900 | bytes 917623 | solution.py:296
  717.3 4.4 collective-permute-start
  724.6 4.4 collective-permute-start
  738.4 8.0 %while.43 = (s32[]{:T(128)}, f32[8,256]{1,0:T(8,128)S(1)}, f32[8,256]{1,0:T(8,128)S(1)}, f32[8,256,64]{1,2,0:T(8,128)S(1)}, s32[4]{0:T(128)S(1)}, /*index=5*/s32...) while((s32[]{:T(128)}, f32[8,256]{1,0:T(8,128)S(1)}, ...), condition=%wide.region_9.10_spmd.clone, body=%wide.region_4.9_spmd.clone.sunk | while | flops 171782656 | bytes 8665903 | solution.py:185
  752.9 16.3 %reduce-scatter.2.cloned.1.call-done = bf16[128,2048]{1,0:T(8,128)(2,1)} async-done(((bf16[256,2048]{1,0:T(8,128)(2,1)}), bf16[128,2048]{1,0:T(8,128)(2,1)}) %reduce-scatter.2.cloned.1.call-update) | async-done | bytes 524304 | tf_op jit(solution)/shard_map/reduce_scatter | solution.py:322
  (379 shorter events, 218.2 us)
Async XLA Ops:
  7.2 229.0 %copy-start = (bf16[256,512]{1,0:T(8,128)(2,1)S(1)}, bf16[256,512]{1,0:T(8,128)(2,1)}, u32[]{:S(2)}) copy-start(bf16[256,512]{1,0:T(8,128)(2,1)} %param.42) | copy-start | bytes 786436
  7.2 200.1 %copy-start.26 = (bf16[2048,128]{1,0:T(8,128)(2,1)S(1)}, bf16[2048,128]{1,0:T(8,128)(2,1)}, u32[]{:S(2)}) copy-start(bf16[2048,128]{1,0:T(8,128)(2,1)} %param.48) | copy-start | bytes 1572868
  7.2 200.1 %copy-start.27 = (bf16[2048,128]{1,0:T(8,128)(2,1)S(1)}, bf16[2048,128]{1,0:T(8,128)(2,1)}, u32[]{:S(2)}) copy-start(bf16[2048,128]{1,0:T(8,128)(2,1)} %param.53) | copy-start | bytes 1572868
  7.2 14.5 %all-gather.11.cloned.1.call-start = ((), (), s32[]{:S(2)}) async-start(), calls=%async_computation.1 | async-start | bytes 1572864 | tf_op jit(solution)/shard_map/all_gather | solution.py:106
  7.9 43.0 %all-gather.15.cloned.1.call-start = ((), (), s32[]{:S(2)}) async-start(), calls=%async_computation.3 | async-start | bytes 1310720 | tf_op jit(solution)/shard_map/all_gather | solution.py:89
  8.7 79.3 %all-gather.17.cloned.1.call-start = ((), (), s32[]{:S(2)}) async-start(), calls=%async_computation.4 | async-start | bytes 2621440 | tf_op jit(solution)/shard_map/all_gather | solution.py:91
  9.4 115.4 %all-gather.19.cloned.1.call-start = ((), (), s32[]{:S(2)}) async-start(), calls=%async_computation.5 | async-start | bytes 2621440 | tf_op jit(solution)/shard_map/all_gather | solution.py:92
  10.0 151.8 %all-gather.21.cloned.1.call-start = ((), (), s32[]{:S(2)}) async-start(), calls=%async_computation.6 | async-start | bytes 2621440 | tf_op jit(solution)/shard_map/all_gather | solution.py:93
  10.6 196.7 %all-gather.13.cloned.1.call-start = ((), (), s32[]{:S(2)}) async-start(), calls=%async_computation.2 | async-start | bytes 3932160 | tf_op jit(solution)/shard_map/all_gather | solution.py:88
  11.2 723.2 %all-gather.25.cloned.1.call-start = ((), (), s32[]{:S(2)}) async-start(), calls=%async_computation.8 | async-start | bytes 1310720 | tf_op jit(solution)/shard_map/all_gather | solution.py:148
  23.2 203.5 %copy-start.20 = (bf16[1,256,2048]{2,1,0:T(8,128)(2,1)S(1)}, bf16[1,256,2048]{2,1,0:T(8,128)(2,1)}, u32[]{:S(2)}) copy-start(bf16[1,256,2048]{2,1,0:T(8,128)(2,1)} %all-gather.11.cloned.1.call-done) | copy-start | bytes 3145732
  23.2 203.5 %copy-start.46 = (f32[2048]{0:T(1024)S(1)}, f32[2048]{0:T(1024)}, u32[]{:S(2)}) copy-start(f32[2048]{0:T(1024)} %param.36) | copy-start | bytes 24580
  237.4 499.3 %all-gather.23.cloned.1.call-start = ((), (), s32[]{:S(2)}) async-start(), calls=%async_computation.7 | async-start | bytes 1966080 | tf_op jit(solution)/shard_map/all_gather | solution.py:143
  241.2 505.3 %all-gather.27.cloned.1.call-start = ((), (), s32[]{:S(2)}) async-start(), calls=%async_computation.9 | async-start | bytes 2621440 | tf_op jit(solution)/shard_map/all_gather | solution.py:319
  241.9 506.9 %all-gather.29.cloned.1.call-start = ((), (), s32[]{:S(2)}) async-start(), calls=%async_computation.10 | async-start | bytes 2621440 | tf_op jit(solution)/shard_map/all_gather | solution.py:320
  242.5 526.7 %reduce-scatter.2.cloned.1.call-start = ((), (), s32[]{:S(2)}) async-start(), calls=%async_computation.11 | async-start | bytes 1572864 | tf_op jit(solution)/shard_map/reduce_scatter | solution.py:322
  281.2 30.7 %copy-start.23 = (f32[16,8,16,64]{3,2,1,0:T(8,128)}, f32[16,8,16,64]{3,2,1,0:T(8,128)S(1)}, u32[]{:S(2)}) copy-start(f32[16,8,16,64]{3,2,1,0:T(8,128)S(1)} %copy.77) | copy-start | bytes 1572868
  282.5 29.4 %copy-start.24 = (f32[16,8,16,64]{3,2,1,0:T(8,128)}, f32[16,8,16,64]{3,2,1,0:T(8,128)S(1)}, u32[]{:S(2)}) copy-start(f32[16,8,16,64]{3,2,1,0:T(8,128)S(1)} %copy.82) | copy-start | bytes 1572868
  311.9 30.0 %copy-start.19 = (bf16[256,512]{0,1:T(8,128)(2,1)S(1)}, bf16[256,512]{0,1:T(8,128)(2,1)}, u32[]{:S(2)}) copy-start(bf16[256,512]{0,1:T(8,128)(2,1)} %get-tuple-element.392) | copy-start | bytes 786436
  311.9 30.4 %copy-start.40 = (pred[16,16]{1,0:T(8,128)(4,1)S(1)}, pred[16,16]{1,0:T(8,128)(4,1)}, u32[]{:S(2)}) copy-start(pred[16,16]{1,0:T(8,128)(4,1)} %iota_compare_fusion.3) | copy-start | bytes 772
  361.0 179.2 %copy-start.13 = (bf16[256,512]{0,1:T(8,128)(2,1)S(1)}, bf16[256,512]{0,1:T(8,128)(2,1)}, u32[]{:S(2)}) copy-start(bf16[256,512]{0,1:T(8,128)(2,1)} %get-tuple-element.393) | copy-start | bytes 786436
  710.9 6.0 collective-permute-start
  717.3 6.9 collective-permute-start
  724.6 6.9 collective-permute-start
  (39 other events, 438.6 us)
Sparse Core Ops, SparseCore 0:
  9.6 11.7 all-gather.10
  23.2 27.6 all-gather.14
  52.7 35.1 all-gather.16
  89.6 35.1 all-gather.18
  126.5 35.1 all-gather.20
  163.4 43.8 all-gather.12
  237.5 29.9 all-gather.24
  269.1 35.9 all-gather.22
  307.0 33.2 all-gather.26
  341.9 35.0 all-gather.28
  752.4 16.7 reduce-scatter.1
where the time goes:
time: 787 us; the launch traced here: 776 us
  matrix products  259 us (33%)
  waiting for transfers between devices  213 us (27%)
  other arithmetic  179 us (23%)
  local copies, waits for them, and re-layouts  69.4 us (9%)
  starting transfers between devices  25.6 us (3%)
  between operations  15.1 us (2%)
  blocking collectives  10.1 us (1%)
    another operation x5, other arithmetic, shards(): lax.linalg.triangular_solve(system, start_coef, left_side=True, lower=Tru...  162 us
    all_gather x1, waiting for transfers between devices, shards(): lax.all_gather(question_projection, 'fs', axis=0, tiled=True)  45.6 us
    all_gather x1, waiting for transfers between devices, shards(): lax.all_gather(acceptance_projection, 'fs', axis=0, tiled=True)  37.1 us
    all_gather x1, waiting for transfers between devices, shards(): lax.all_gather(state_address_projection, 'fs', axis=0, tiled=True)  36.9 us
    all_gather x1, waiting for transfers between devices, shards(): lax.all_gather(state_content_projection, 'fs', axis=0, tiled=True)  36.9 us
    dot_general x1, matrix products, shards(): jnp.einsum('nhtsk,nhsk,nhtk->nhts', before, span_key, toward, precision=h...  30 us
    dot_general x1, matrix products, shards(): jnp.einsum('nhtsk,nhsk,nhtk->nhts', before, remove, toward, precision=hig...  29.4 us
    dot_general x16, matrix products, advance(): jnp.einsum('hvk,htk->htv', local_now, coef_here, precision=highest)  29 us
  transfers between devices with their start and end apart: 14, of which 9 were waited for; matrix products, arithmetic and copies ran while one was open for 61% of the time, Pallas kernels for 0%

commit v1 on v0

v1 whole, which is shorter than its diff:
```python
import jax
import jax.numpy as jnp
from jax import lax
from jax.experimental import pallas as pl
from jax.experimental.pallas import tpu as pltpu
from jax.sharding import PartitionSpec as P

NOPE = 64
ROPE = 32
VHEAD = 64
BRANCH_CHANNELS = 64
TOK_DEV = 256


norm_epsilon = 1e-06
group_epsilon = 0.00064
highest = lax.Precision.HIGHEST


def rms_rows(values, gain):
    floats = values.astype(jnp.float32)
    return (
        floats * lax.rsqrt(jnp.mean(floats * floats, axis=-1, keepdims=True) + norm_epsilon) * gain
    )


def rotate(values, positions):
    half = values.shape[-1] // 2
    inverse = 10000.0 ** (-jnp.arange(half, dtype=jnp.float32) / half)
    angle = positions.astype(jnp.float32)[:, None] * inverse[None, :]
    cosine = jnp.cos(angle)[:, None, :]
    sine = jnp.sin(angle)[:, None, :]
    first = values[..., :half]
    second = values[..., half:]
    return jnp.concatenate(
        [first * cosine - second * sine, second * cosine + first * sine], axis=-1
    )


def finish(stacked, gain, positions):
    normed = rms_rows(stacked, gain)
    return jnp.concatenate(
        [normed[..., :NOPE], rotate(normed[..., NOPE:], positions)], axis=-1
    ).astype(jnp.bfloat16)


def matmul(left, right):
    return jnp.dot(left, right, preferred_element_type=jnp.float32)


def mxu(left, right, contract):
    return lax.dot_general(
        left.astype(jnp.bfloat16),
        right.astype(jnp.bfloat16),
        ((contract[0], contract[1]), ((), ())),
        preferred_element_type=jnp.float32,
    )


plain = ((1,), (0,))
by_lanes = ((1,), (1,))
by_rows = ((0,), (0,))


def split_heads(values):
    width = values.shape[1]
    lane = lax.broadcasted_iota(jnp.int32, values.shape, 1)
    low = lane < width // 2
    return jnp.concatenate([jnp.where(low, values, 0.0), jnp.where(low, 0.0, values)], axis=0)


def head_sums(values):
    lane = lax.broadcasted_iota(jnp.int32, values.shape, 1)
    low = lane < values.shape[1] // 2
    first = jnp.sum(jnp.where(low, values, 0.0), axis=-1, keepdims=True)
    second = jnp.sum(jnp.where(low, 0.0, values), axis=-1, keepdims=True)
    return jnp.where(low, first, second)


def chunk_kernel(
    recept_ref, key_ref, value_ref, log_ref, learn_ref, free_ref, along_ref, state_ref
):
    rows, width = log_ref.shape
    size = BRANCH_CHANNELS
    chunks = rows // size
    row = lax.broadcasted_iota(jnp.int32, (size, width), 0)
    col = lax.broadcasted_iota(jnp.int32, (size, width), 1) & (size - 1)
    strict = row > col
    inclusive = row >= col
    tri = (
        lax.broadcasted_iota(jnp.int32, (size, size), 0)
        >= lax.broadcasted_iota(jnp.int32, (size, size), 1)
    ).astype(jnp.float32)
    wide_row = lax.broadcasted_iota(jnp.int32, (width, width), 0)
    wide_col = lax.broadcasted_iota(jnp.int32, (width, width), 1)
    same_head = (wide_row < size) == (wide_col < size)
    state = jnp.zeros((width, width), jnp.float32)
    along = (wide_row == wide_col).astype(jnp.float32)
    for chunk in range(chunks):
        here = pl.ds(chunk * size, size)
        log_decay = log_ref[here, :]
        cum = lax.dot_general(
            tri,
            log_decay,
            (((1,), (0,)), ((), ())),
            precision=highest,
            preferred_element_type=jnp.float32,
        )
        prev = cum - log_decay
        middle = cum[size // 2 - 1 : size // 2, :]
        end = cum[size - 1 : size, :]
        key = key_ref[here, :].astype(jnp.float32)
        value = value_ref[here, :].astype(jnp.float32)
        recept = recept_ref[here, :].astype(jnp.float32)
        unit = key * lax.rsqrt(head_sums(key * key) + 1e-06)
        remove = unit * learn_ref[here, :]
        grow = jnp.exp(middle - cum)
        left = jnp.concatenate([-unit * jnp.exp(prev - middle), recept * jnp.exp(cum - middle)], 0)
        right = jnp.concatenate([split_heads(remove * grow), split_heads(key * grow)], 0)
        pairs = mxu(left, right, by_lanes)
        remove_before = jnp.where(strict, pairs[:size, :width], 0.0)
        key_before = jnp.where(strict, pairs[:size, width:], 0.0)
        remove_upto = jnp.where(inclusive, pairs[size:, :width], 0.0)
        key_upto = jnp.where(inclusive, pairs[size:, width:], 0.0)
        inverse = (row == col).astype(jnp.float32) + jnp.where(
            (row >> 1) == (col >> 1), remove_before, 0.0
        )
        level = 1
        while (1 << level) < size:
            joins = ((row >> (level + 1)) == (col >> (level + 1))) & (
                (row >> level) != (col >> level)
            )
            inner = mxu(jnp.where(joins, remove_before, 0.0), split_heads(inverse), plain)
            inverse = inverse + mxu(inverse, split_heads(inner), plain)
            level += 1
        from_keys = mxu(
            jnp.concatenate([key_before, key_upto], 0), split_heads(value), plain
        )
        lead = mxu(
            inverse,
            jnp.concatenate(
                [split_heads(-unit * jnp.exp(prev)), split_heads(from_keys[:size])], 1
            ),
            plain,
        )
        lead_coef = lead[:, :width]
        lead_free = lead[:, width:]
        reads = mxu(
            remove_upto,
            jnp.concatenate([split_heads(lead_coef), split_heads(lead_free)], 1),
            plain,
        )
        coef = recept * jnp.exp(cum) + reads[:, :width]
        free = reads[:, width:] + from_keys[size:]
        tail = jnp.exp(end - cum)
        remove_tail = remove * tail
        step_map = jnp.where(same_head, mxu(lead_coef, remove_tail, by_rows), 0.0)
        step_add = jnp.where(
            same_head,
            mxu(
                jnp.concatenate([lead_free, value], 0),
                jnp.concatenate([remove_tail, key * tail], 0),
                by_rows,
            ),
            0.0,
        )
        both = jnp.concatenate([state, along], 0)
        read = mxu(coef, both, by_lanes)
        free_ref[here, :] = free + read[:, :width]
        along_ref[here, :] = read[:, width:]
        moved = both * jnp.exp(end) + mxu(both, step_map, plain)
        state = moved[:width] + step_add
        along = moved[width:]
    state_ref[0] = (along[:size] + along[size:]).astype(state_ref.dtype)
    state_ref[1] = (state[:size] + state[size:]).astype(state_ref.dtype)


def finish_kernel(
    place_ref, states_ref, free_ref, along_ref, recept_ref, key_ref, value_ref,
    present_ref, gain_ref, out_ref,
):
    place = place_ref[0]
    width = free_ref.shape[1]
    entering = jnp.zeros((width, width), jnp.float32)
    for other in range(states_ref.shape[0] - 1):
        transfer = split_heads(states_ref[other, 0].astype(jnp.float32))
        local = split_heads(states_ref[other, 1].astype(jnp.float32))
        advanced = mxu(entering, transfer, plain) + local
        entering = jnp.where(other < place, advanced, entering)
    read = free_ref[...] + mxu(along_ref[...], entering, by_lanes)
    center = head_sums(read) * (1.0 / BRANCH_CHANNELS)
    spread = head_sums(jnp.square(read - center)) * (1.0 / BRANCH_CHANNELS)
    rescaled = (read - center) * lax.rsqrt(spread + group_epsilon) * gain_ref[...]
    recept = recept_ref[...].astype(jnp.float32)
    key = key_ref[...].astype(jnp.float32)
    value = value_ref[...].astype(jnp.float32)
    own = head_sums(recept * key * present_ref[...]) * value
    out_ref[...] = (rescaled + own).astype(out_ref.dtype)


def recurrence(projected, offsets, log_decay, learn, present, gain):
    rows, total = log_decay.shape
    size = BRANCH_CHANNELS
    width = 2 * size
    groups = total // width

    def piece(offset):
        return pl.BlockSpec((rows, width), lambda i, first=offset // width: (0, first + i))

    spec = pl.BlockSpec((rows, width), lambda i: (0, i))
    vec = pl.BlockSpec((1, width), lambda i: (0, i))
    pieces = [piece(offset) for offset in offsets]
    free, along, states = pl.pallas_call(
        chunk_kernel,
        grid=(groups,),
        in_specs=pieces + [spec, spec],
        out_specs=[spec, spec, pl.BlockSpec((2, size, width), lambda i: (0, 0, i))],
        out_shape=[
            jax.ShapeDtypeStruct((rows, total), jnp.float32),
            jax.ShapeDtypeStruct((rows, total), jnp.float32),
            jax.ShapeDtypeStruct((2, size, total), jnp.bfloat16),
        ],
        cost_estimate=pl.CostEstimate(
            flops=groups * rows * width * width * 40, bytes_accessed=rows * total * 20, transcendentals=0
        ),
        name="chunks",
    )(projected, projected, projected, log_decay, learn)
    everyone = lax.all_gather(states, "sp", axis=0)
    place = lax.axis_index("sp").astype(jnp.int32).reshape(1)
    return pl.pallas_call(
        finish_kernel,
        grid=(groups,),
        in_specs=[
            pl.BlockSpec(memory_space=pltpu.SMEM),
            pl.BlockSpec((everyone.shape[0], 2, size, width), lambda i: (0, 0, 0, i)),
            spec,
            spec,
        ]
        + pieces
        + [vec, vec],
        out_specs=spec,
        out_shape=jax.ShapeDtypeStruct((rows, total), jnp.bfloat16),
        cost_estimate=pl.CostEstimate(
            flops=groups * rows * width * width * 8, bytes_accessed=rows * total * 16, transcendentals=0
        ),
        name="finish",
    )(place, everyone, free, along, projected, projected, projected, present, gain)


def shards(
    layer_entering_vectors,
    entering_rms_coefficients,
    question_projection,
    compressing_projection,
    spinning_address_projection,
    compact_rms_coefficients,
    compact_to_plain_address,
    compact_to_content,
    question_rms_coefficients,
    address_rms_coefficients,
    acceptance_projection,
    state_address_projection,
    state_content_projection,
    fading_first_lowrank,
    fading_second_lowrank,
    fading_channel_bias,
    fading_speed_multiplier,
    fading_extra_exponent,
    adaptation_first_lowrank,
    adaptation_second_lowrank,
    adaptation_channel_bias,
    present_token_coefficients,
    branch_rms_coefficients,
    softmax_merge_projection,
    state_merge_projection,
):
    recur_width = acceptance_projection.shape[1]
    recur_weights = lax.all_gather(
        jnp.concatenate(
            [acceptance_projection, state_address_projection, state_content_projection], axis=1
        ),
        "fs",
        axis=0,
        tiled=True,
    )
    attend_weights = lax.all_gather(
        jnp.concatenate(
            [compressing_projection, question_projection, spinning_address_projection], axis=1
        ),
        "fs",
        axis=0,
        tiled=True,
    )
    normed = rms_rows(
        lax.all_gather(layer_entering_vectors, "tp", axis=1, tiled=True)[0],
        entering_rms_coefficients,
    ).astype(jnp.bfloat16)
    decay_in = matmul(normed, fading_first_lowrank).astype(jnp.bfloat16)
    rate_low = matmul(normed, adaptation_first_lowrank).astype(jnp.bfloat16)
    recur_in = matmul(normed, recur_weights).astype(jnp.bfloat16)
    projected = matmul(normed, attend_weights).astype(jnp.bfloat16)
    latent_width = compressing_projection.shape[1]
    latent = projected[:, :latent_width]
    query = projected[:, latent_width : latent_width + question_projection.shape[1]]
    rope_key = projected[:, latent_width + question_projection.shape[1] :]
    row_count = projected.shape[0]
    attn_heads = compact_to_plain_address.shape[1] // NOPE
    qk_size = NOPE + ROPE
    own_positions = lax.axis_index("sp") * row_count + jnp.arange(row_count, dtype=jnp.int32)
    last_position = lax.axis_index("sp") * row_count + row_count - 1
    latent_normed = rms_rows(latent, compact_rms_coefficients).astype(jnp.bfloat16)
    query_ready = finish(
        query.reshape(row_count, attn_heads, qk_size), question_rms_coefficients, own_positions
    )
    scale = qk_size ** (-0.5)
    start_carry = (
        jnp.full((attn_heads, row_count), -jnp.inf, jnp.float32),
        jnp.zeros((attn_heads, row_count), jnp.float32),
        jnp.zeros((attn_heads, row_count, VHEAD), jnp.float32),
    )
    length_here = latent_normed.shape[0]
    key_nope = (
        matmul(latent_normed, compact_to_plain_address)
        .astype(jnp.bfloat16)
        .reshape(length_here, attn_heads, NOPE)
    )
    values_here = (
        matmul(latent_normed, compact_to_content)
        .astype(jnp.bfloat16)
        .reshape(length_here, attn_heads, VHEAD)
    )
    key_stack = jnp.concatenate(
        [key_nope, jnp.broadcast_to(rope_key[:, None, :], (length_here, attn_heads, ROPE))], axis=-1
    )
    key_ready = finish(key_stack, address_rms_coefficients, own_positions)
    carry = start_carry
    key_rows = lax.all_gather(key_ready, "sp", axis=0, tiled=True)
    length_here = key_rows.shape[0]
    block = TOK_DEV
    blocks = length_here // block
    keys_blocked = key_rows.reshape(blocks, block, attn_heads, qk_size)
    values_blocked = lax.all_gather(values_here, "sp", axis=0, tiled=True).reshape(
        blocks, block, attn_heads, VHEAD
    )

    def visit(state, inputs):
        key_block, value_block, index = inputs
        block_start = index * block

        def compute(running):
            running_max, running_total, running_sum = running
            scores = (
                jnp.einsum(
                    "qhd,khd->hqk", query_ready, key_block, preferred_element_type=jnp.float32
                )
                * scale
            )
            key_positions = block_start + jnp.arange(block, dtype=jnp.int32)
            allowed = key_positions[None, :] <= own_positions[:, None]
            scores = jnp.where(allowed[None], scores, -jnp.inf)
            new_max = jnp.maximum(running_max, jnp.max(scores, axis=-1))
            safe_max = jnp.where(jnp.isfinite(new_max), new_max, 0.0)
            weights = jnp.exp(scores - safe_max[..., None])
            factor = jnp.exp(running_max - safe_max)
            new_total = running_total * factor + jnp.sum(weights, axis=-1)
            new_sum = running_sum * factor[..., None] + jnp.einsum(
                "hqk,khd->hqd",
                weights.astype(jnp.bfloat16),
                value_block,
                preferred_element_type=jnp.float32,
            )
            return (new_max, new_total, new_sum)

        def keep(running):
            return running

        return (lax.cond(block_start > last_position, keep, compute, state), None)

    carry, _ = lax.scan(
        visit, carry, (keys_blocked, values_blocked, jnp.arange(blocks, dtype=jnp.int32))
    )
    final_max, final_total, final_sum = carry
    attended = (final_sum / final_total[..., None]).astype(jnp.bfloat16)
    attended = jnp.transpose(attended, (1, 0, 2)).reshape(row_count, attn_heads * VHEAD)
    log_total = final_max + jnp.log(final_total)
    recurrent_heads = fading_second_lowrank.shape[1] // BRANCH_CHANNELS

    decay_low = jnp.tanh(decay_in.astype(jnp.float32)).astype(jnp.bfloat16)
    rate_logarithm = (
        -jax.nn.softplus(-(fading_channel_bias + matmul(decay_low, fading_second_lowrank))) - 0.5
    )
    log_decay = (
        -jnp.exp(rate_logarithm).reshape(row_count, recurrent_heads, BRANCH_CHANNELS)
        * jnp.transpose(fading_speed_multiplier[0])[:, :, None]
        + jnp.transpose(fading_extra_exponent[0])[:, :, None]
    )
    learn = jax.nn.sigmoid(adaptation_channel_bias + matmul(rate_low, adaptation_second_lowrank))
    state_branch_result = recurrence(
        recur_in,
        (0, recur_width, 2 * recur_width),
        log_decay.reshape(row_count, recur_width),
        learn,
        present_token_coefficients.reshape(1, recur_width),
        branch_rms_coefficients.reshape(1, recur_width),
    )
    out_attn_full, out_rec_full = (
        lax.all_gather(softmax_merge_projection, "fs", axis=1, tiled=True),
        lax.all_gather(state_merge_projection, "fs", axis=1, tiled=True),
    )
    mixed = lax.psum_scatter(
        (matmul(attended, out_attn_full) + matmul(state_branch_result, out_rec_full)).astype(
            jnp.bfloat16
        ),
        "tp",
        scatter_dimension=0,
        tiled=True,
    )
    return (mixed[None], log_total[None])


def solution(mesh):
    placed = (
        P("fs", ("sp", "tp"), None),
        P(),
        P("fs", "tp"),
        P("fs", None),
        P("fs", None),
        P(),
        P(None, "tp"),
        P(None, "tp"),
        P(),
        P(),
        P("fs", "tp"),
        P("fs", "tp"),
        P("fs", "tp"),
        P(),
        P(None, "tp"),
        P("tp"),
        P("fs", "tp", "sp"),
        P("fs", "tp", "sp"),
        P(),
        P(None, "tp"),
        P("tp"),
        P("tp", None),
        P("tp"),
        P("tp", "fs"),
        P("tp", "fs"),
    )
    return jax.shard_map(
        shards,
        mesh=mesh,
        in_specs=placed,
        out_specs=(P("fs", ("sp", "tp"), None), P("fs", "tp", "sp")),
        check_vma=False,
    )
```

time: 787 us -> 343 us (0.44); the launches traced: 776 us -> 342 us
  matrix products: 259 us -> 24.3 us
  other arithmetic: 179 us -> 7.72 us
  local copies, waits for them, and re-layouts: 69.4 us -> 10.6 us
  Pallas kernels: 0 us -> 39.1 us
  starting transfers between devices: 25.6 us -> 0.5 us
  waiting for transfers between devices: 213 us -> 225 us
    dot_general x79 -> x0, matrix products: 233 us -> none  [the longest x1 30 us: shards(): jnp.einsum('nhtsk,nhsk,nhtk->nhts', before, span_key, toward, precision=h...]
    another operation x9 -> x1, other arithmetic: 165 us -> 0.07 us  [the longest x5 162 us: shards(): lax.linalg.triangular_solve(system, start_coef, left_side=True, lower=Tru...]
    all_gather x5 -> x2, waiting for transfers between devices: 184 us -> 128 us  [the longest x1 69.4 us: shards(): lax.all_gather(jnp.concatenate([acceptance_projection, state_address_proj...]
    pallas_call x0 -> x2, Pallas kernels: none -> 39.1 us  [the longest x1 33.9 us: recurrence(): pl.pallas_call(chunk_kernel, grid=(groups,), in_specs=pieces + [spec, spe...]
    all_gather x1, waiting for transfers between devices: 0.01 us -> 35.1 us  [shards(): key_rows = lax.all_gather(key_ready, 'sp', axis=0, tiled=True)]
    all_gather x1, waiting for transfers between devices: 0.02 us -> 25.3 us  [shards(): lax.all_gather(softmax_merge_projection, 'fs', axis=1, tiled=True)]
    concatenate x1 -> x0, local copies, waits for them, and re-layouts: 19.4 us -> none  [shards(): jnp.concatenate(list(gathered) + [fading_first_lowrank, adaptation_first_...]
    dynamic_slice x32 -> x0, local copies, waits for them, and re-layouts: 17.5 us -> none  [shards(): lax.scan(advance, (jnp.zeros_like(identity), identity), (span_map, span_a...]
  transfers between devices with their start and end apart: 14 -> 8, of which waited for: 9 -> 7; matrix products, arithmetic and copies ran while one was open for 61% -> 10% of each run, Pallas kernels for 0% -> 11%
where the time goes in v1:
time: 343 us; the launch traced here: 342 us
  waiting for transfers between devices  225 us (66%)
  Pallas kernels  39.1 us (11%)
  matrix products  24.3 us (7%)
  blocking collectives  17.4 us (5%)
  between operations  14.6 us (4%)
  local copies, waits for them, and re-layouts  10.6 us (3%)
  other arithmetic  7.72 us (2%)
    all_gather x1, waiting for transfers between devices, shards(): lax.all_gather(jnp.concatenate([acceptance_projection, state_address_proj...  69.4 us
    all_gather x1, waiting for transfers between devices, shards(): lax.all_gather(jnp.concatenate([compressing_projection, question_projecti...  58.4 us
    all_gather x1, waiting for transfers between devices, shards(): key_rows = lax.all_gather(key_ready, 'sp', axis=0, tiled=True)  35.1 us
    pallas_call x1, Pallas kernels, recurrence(): pl.pallas_call(chunk_kernel, grid=(groups,), in_specs=pieces + [spec, spe...  33.9 us
    all_gather x1, waiting for transfers between devices, shards(): lax.all_gather(softmax_merge_projection, 'fs', axis=1, tiled=True)  25.3 us
    dot_general x8, matrix products, matmul(): return jnp.dot(left, right, preferred_element_type=jnp.float32)  22.3 us
    all_gather x1, waiting for transfers between devices, shards(): lax.all_gather(values_here, 'sp', axis=0, tiled=True)  17.5 us
    all_gather x1, blocking collectives, recurrence(): everyone = lax.all_gather(states, 'sp', axis=0)  17.4 us
  transfers between devices with their start and end apart: 8, of which 7 were waited for; matrix products, arithmetic and copies ran while one was open for 10% of the time, Pallas kernels for 11%

profile of v1, /device:TPU:0, one launch (start us, length us, event | category | flops | bytes accessed | tf_op | source)
XLA Modules:
  0.0 341.8 jit_solution(17938334689403599527)
XLA Ops:
  8.9 2.3 pad_maximum_fusion.1
  11.3 10.0 %all-gather.9.cloned.1.call-done = bf16[1,256,2048]{2,1,0:T(8,128)(2,1)} async-done(((bf16[1,128,2048]{2,1,0:T(8,128)(2,1)}), bf16[1,256,2048]{2,1,0:T(8,128)(2,1)}) %all-gather.9.cloned.1.call-update) | async-done | bytes 1048592 | tf_op jit(solution)/shard_map/all_gather | solution.py:295
  21.3 1.5 fusion.13
  22.9 58.4 %all-gather.11.cloned.1.call-done = bf16[2048,1056]{1,0:T(8,128)(2,1)} async-done(((bf16[512,1056]{1,0:T(8,128)(2,1)}), bf16[2048,1056]{1,0:T(8,128)(2,1)}) %all-gather.11.cloned.1.call-update) | async-done | bytes 4325392 | tf_op jit(solution)/shard_map/all_gather | solution.py:286
  81.3 4.6 %convolution_convert_fusion.1 = bf16[256,1056]{0,1:T(8,128)(2,1)S(1)} fusion(bf16[2048,1056]{1,0:T(8,128)(2,1)} %all-gather.11.cloned.1.call-done, bf16[1,256,2048]{2,1,0:T(8,128)(2,1)} %all-gather.9.cloned.1.call-done, f32[2048]{0:T(1024)S(1)} %copy-done.13, f32[256]{0:T(256)S(1)} %add_rsqrt_fusion.3), kind=kOutput, calls=%fused_computation.24 | convolution fusion | flops 1109663744 | bytes 5923840 | tf_op jit(solution)/shard_map/dot_general | solution.py:48
  90.2 1.2 pad_maximum_fusion
  94.4 2.5 fusion.20.learn_ref
  96.9 2.9 fusion.33.log_ref
  99.9 17.5 %all-gather.15.cloned.1.call-done = bf16[1024,8,64]{0,2,1:T(8,128)(2,1)} async-done(((bf16[256,8,64]{0,2,1:T(8,128)(2,1)}), bf16[1024,8,64]{0,2,1:T(8,128)(2,1)}) %all-gather.15.cloned.1.call-update) | async-done | bytes 1048592 | tf_op jit(solution)/shard_map/all_gather | solution.py:342
  117.4 2.4 copy.54
  119.7 35.1 %all-gather.13.cloned.1.call-done = bf16[1024,8,96]{0,2,1:T(8,128)(2,1)} async-done(((bf16[256,8,96]{0,2,1:T(8,128)(2,1)}), bf16[1024,8,96]{0,2,1:T(8,128)(2,1)}) %all-gather.13.cloned.1.call-update) | async-done | bytes 1572880 | tf_op jit(solution)/shard_map/all_gather | solution.py:337
  154.8 1.6 copy.53
  156.5 7.9 %while.15 = (s32[]{:T(128)}, f32[8,256]{1,0:T(8,128)S(1)}, f32[8,256]{1,0:T(8,128)S(1)}, f32[8,256,64]{1,2,0:T(8,128)S(1)}, s32[4]{0:T(128)S(1)}, /*index=5*/s32...) while((s32[]{:T(128)}, f32[8,256]{1,0:T(8,128)S(1)}, ...), condition=%wide.region_9.10_spmd.clone, body=%wide.region_4.9_spmd.clone.sunk | while | flops 171782656 | bytes 8665895 | solution.py:379
  157.8 2.5 conditional.3
  158.8 1.5 convolution_add_fusion
  164.4 25.3 %all-gather.17.cloned.1.call-done = bf16[512,2048]{1,0:T(8,128)(2,1)} async-done(((bf16[512,512]{1,0:T(8,128)(2,1)}), bf16[512,2048]{1,0:T(8,128)(2,1)}) %all-gather.17.cloned.1.call-update) | async-done | bytes 2097168 | tf_op jit(solution)/shard_map/all_gather | solution.py:407
  189.8 2.3 fusion.46
  192.1 69.4 %all-gather.19.cloned.1.call-done = bf16[2048,1536]{1,0:T(8,128)(2,1)} async-done(((bf16[512,1536]{1,0:T(8,128)(2,1)}), bf16[2048,1536]{1,0:T(8,128)(2,1)}) %all-gather.19.cloned.1.call-update) | async-done | bytes 6291472 | tf_op jit(solution)/shard_map/all_gather | solution.py:278
  261.5 5.9 %convolution_convert_fusion.recept_ref.key_ref.value_ref = bf16[256,1536]{1,0:T(8,128)(2,1)} fusion(bf16[2048,1536]{1,0:T(8,128)(2,1)} %all-gather.19.cloned.1.call-done, bf16[1,256,2048]{2,1,0:T(8,128)(2,1)} %all-gather.9.cloned.1.call-done, f32[2048]{0:T(1024)S(1)} %copy-done.14, f32[256]{0:T(256)S(1)} %add_rsqrt_fusion.3), kind=kOutput, calls=%fused_computation.23 | convolution fusion | flops 1613103104 | bytes 8135680 | tf_op jit(solution)/shard_map/dot_general | solution.py:48
  267.5 33.9 %chunks.1 = (f32[256,512]{1,0:T(8,128)}, f32[256,512]{1,0:T(8,128)}, bf16[2,64,512]{2,1,0:T(8,128)(2,1)}) custom-call(bf16[256,1536]{1,0:T(8,128)(2,1)} %convolution_convert_fusion.recept_ref.key_ref.value_ref, bf16[256,1536]{1,0:T(8,128)(2,1)} %convolution_convert_fusion.recept_ref.key_ref.value_ref, ...), custom_call_target="tpu_custom_call" | custom-call | flops 671088640 | bytes 2621440 | tf_op jit(solution)/shard_map/chunks/pallas_call | solution.py:213
  301.3 17.4 %all-gather = bf16[8,64,512]{2,1,0:T(8,128)(2,1)} all-gather(bf16[2,64,512]{2,1,0:T(8,128)(2,1)} %get-tuple-element.144), channel_id=2, replica_groups=mesh['sp'=4,'fs'=4,'tp'=2] {'sp'}, dimensions={0}, use_global_device_ids=true | all-gather | bytes 655360 | tf_op jit(solution)/shard_map/all_gather | solution.py:228
  318.8 5.3 %finish.1 = bf16[256,512]{1,0:T(8,128)(2,1)} custom-call(s32[1]{0:T(128)} %bitcast.11.place_ref, bf16[4,2,64,512]{3,2,1,0:T(8,128)(2,1)} %bitcast.71, f32[256,512]{1,0:T(8,128)} %get-tuple-element.145.free_ref, f32[256,512]{1,0:T(8,128)} %get-tuple-element.146.along_ref, bf16[256,1536]{1,0:T(8,128)(2,1)} %convolution_convert_fusion.recept_ref.key_ref.value_ref, ...), custom_call_target="tpu_custom_call" | custom-call | flops 134217728 | bytes 2097152 | tf_op jit(solution)/shard_map/finish/pallas_call | solution.py:230
  324.0 3.4 fusion.12
  328.1 6.9 %reduce-scatter.2.cloned.1.call-done = bf16[128,2048]{1,0:T(8,128)(2,1)} async-done(((bf16[256,2048]{1,0:T(8,128)(2,1)}), bf16[128,2048]{1,0:T(8,128)(2,1)}) %reduce-scatter.2.cloned.1.call-update) | async-done | bytes 524304 | tf_op jit(solution)/shard_map/reduce_scatter | solution.py:410
  (110 shorter events, 13.1 us)
Async XLA Ops:
  7.2 87.2 %copy-start = (bf16[2048,128]{1,0:T(8,128)(2,1)S(1)}, bf16[2048,128]{1,0:T(8,128)(2,1)}, u32[]{:S(2)}) copy-start(bf16[2048,128]{1,0:T(8,128)(2,1)} %param.47) | copy-start | bytes 1572868
  7.2 14.1 %all-gather.9.cloned.1.call-start = ((), (), s32[]{:S(2)}) async-start(), calls=%async_computation.1 | async-start | bytes 1572864 | tf_op jit(solution)/shard_map/all_gather | solution.py:295
  7.9 73.4 %all-gather.11.cloned.1.call-start = ((), (), s32[]{:S(2)}) async-start(), calls=%async_computation.2 | async-start | bytes 5898240 | tf_op jit(solution)/shard_map/all_gather | solution.py:286
  8.8 72.5 %copy-start.13 = (f32[2048]{0:T(1024)S(1)}, f32[2048]{0:T(1024)}, u32[]{:S(2)}) copy-start(f32[2048]{0:T(1024)} %param.30) | copy-start | bytes 24580
  11.2 106.1 %all-gather.15.cloned.1.call-start = ((), (), s32[]{:S(2)}) async-start(), calls=%async_computation.4 | async-start | bytes 1310720 | tf_op jit(solution)/shard_map/all_gather | solution.py:342
  22.8 63.2 %copy-start.11 = (bf16[256,512]{1,0:T(8,128)(2,1)S(1)}, bf16[256,512]{1,0:T(8,128)(2,1)}, u32[]{:S(2)}) copy-start(bf16[256,512]{1,0:T(8,128)(2,1)} %param.36) | copy-start | bytes 786436
  22.8 63.2 %copy-start.16 = (f32[256]{0:T(256)S(1)}, f32[256]{0:T(256)}, u32[]{:S(2)}) copy-start(f32[256]{0:T(256)} %param.34) | copy-start | bytes 3076
  85.9 1.6 copy-start.12
  86.0 2.2 copy-start.9
  86.0 2.2 copy-start.10
  87.3 67.5 %all-gather.13.cloned.1.call-start = ((), (), s32[]{:S(2)}) async-start(), calls=%async_computation.3 | async-start | bytes 1966080 | tf_op jit(solution)/shard_map/all_gather | solution.py:337
  88.5 1.6 copy-start.3
  88.5 1.6 copy-start.4
  88.5 1.6 copy-start.5
  89.5 100.3 %all-gather.17.cloned.1.call-start = ((), (), s32[]{:S(2)}) async-start(), calls=%async_computation.5 | async-start | bytes 2621440 | tf_op jit(solution)/shard_map/all_gather | solution.py:407
  90.1 2.4 copy-start.6
  90.1 171.5 %all-gather.19.cloned.1.call-start = ((), (), s32[]{:S(2)}) async-start(), calls=%async_computation.6 | async-start | bytes 7864320 | tf_op jit(solution)/shard_map/all_gather | solution.py:278
  91.4 2.3 copy-start.8
  91.4 3.0 copy-start.1
  91.5 232.6 %all-gather.21.cloned.1.call-start = ((), (), s32[]{:S(2)}) async-start(), calls=%async_computation.7 | async-start | bytes 2621440 | tf_op jit(solution)/shard_map/all_gather | solution.py:408
  92.2 242.8 %reduce-scatter.2.cloned.1.call-start = ((), (), s32[]{:S(2)}) async-start(), calls=%async_computation.8 | async-start | bytes 1572864 | tf_op jit(solution)/shard_map/reduce_scatter | solution.py:410
  94.4 2.5 copy-start.2
  94.4 2.5 copy-start.14
  94.4 2.5 copy-start.15
  (1 other events, 1.3 us)
Sparse Core Ops, SparseCore 0:
  9.5 11.7 all-gather.8
  23.2 58.1 all-gather.10
  87.4 29.9 all-gather.14
  118.8 35.9 all-gather.12
  156.5 33.2 all-gather.16
  191.5 70.0 all-gather.18
  263.4 35.8 all-gather.20
  327.6 7.3 reduce-scatter.1
